TPU v7x, 128 devices: a whole 4x4x4 slice. The times are simulated.
128 devices in a mesh: sp: 16 (over z, y), tp: 8 (over x, core).
Axes of the slice: x: 4, y: 4, z: 4, core: 2. Of those that a mesh axis runs over, the one named last changes fastest.
Arguments:
- skip_stream_vector: bfloat16 [16384, 2048], P(('sp', 'tp')), may hold values from -6 to 6
- probe_preactivation: bfloat16 [16384, 1024], P('sp', 'tp'), may hold values from -6 to 6
- retention_preactivation: bfloat16 [16384, 1024], P('sp', 'tp'), may hold values from -4.5 to 4.5
- content_vector: bfloat16 [16384, 1024], P('sp', 'tp'), may hold values from -6 to 6
- emission_preactivation: bfloat16 [16384, 1024], P('sp', 'tp'), may hold values from -6 to 6
- retention_slack: float32 [1024], P('tp'), may hold values from 0 to 0.12
- surge_rate: float32 [16384, 1024], P('sp', 'tp'), may hold values from -1.2 to 0
- subspace_scaling_factor: float32 [1024], P('tp'), may hold values from 0.1 to 1.9
- emission_matrix: bfloat16 [1024, 2048], replicated, may hold values from -0.1875 to 0.1875
- mlp_scaling_factor: float32 [2048], replicated, may hold values from 0.1 to 1.9
- switch_matrix: bfloat16 [2048, 5632], P('sp', 'tp'), may hold values from -0.125 to 0.125
- expansion_matrix: bfloat16 [2048, 5632], P('sp', 'tp'), may hold values from -0.125 to 0.125
- contraction_matrix: bfloat16 [5632, 2048], P('tp', 'sp'), may hold values from -0.078125 to 0.078125
Outputs:
- stream_out: bfloat16 [16384, 2048], P(('sp', 'tp'))
All inputs are finite; a program needn't handle non-finite values.
Results may differ from a plain program's by a relative error of at most 0.017.
Values may be sent and summed in bfloat16 or wider, within the bound.
A program may use at most 128 MiB of HBM per device.

v0:
```python
import jax
import jax.numpy as jnp
from jax import lax
from jax.sharding import Mesh
from jax.sharding import PartitionSpec as P

HEAD_DIM = 128
BLOCK = 64
TP = ("tp_0", "tp_1")
SP_TP = ("sp", "tp_0", "tp_1")
EPSILON = 1e-06
TOP_PRECISION = lax.Precision.HIGHEST


def in_one_piece(arrays, axis, dim, along):
    both = jnp.concatenate(arrays, axis=along)
    whole, at, outs = (lax.all_gather(both, axis, axis=dim, tiled=True), 0, [])
    for a in arrays:
        outs.append(lax.slice_in_dim(whole, at, at + a.shape[along], axis=along))
        at += a.shape[along]
    return tuple(outs)


def from_everyone(value, axis):
    peers = lax.axis_size(axis)
    return lax.all_to_all(
        jnp.broadcast_to(value[None], (peers, *value.shape)), axis, 0, 0, tiled=True
    )


def all_in_one(value, axis):
    leaves = jax.tree.leaves(value)
    order = sorted(range(len(leaves)), key=lambda k: -leaves[k].size)
    width = (1, *leaves[order[0]].shape)[-1]
    lines = [
        jnp.pad(leaves[k].reshape(-1), (0, -leaves[k].size % width)).reshape(-1, width)
        for k in order
    ]
    both, at, found = (from_everyone(jnp.concatenate(lines), axis), 0, {})
    for k, line in zip(order, lines):
        piece = both[:, at : at + len(line)].reshape(len(both), -1)
        found[k] = piece[:, : leaves[k].size].reshape(-1, *leaves[k].shape)
        at += len(line)
    numbers = iter(range(len(leaves)))
    return jax.tree.map(lambda _: found[next(numbers)], value)


def joined_by_halves(pieces, combine):
    while len(jax.tree.leaves(pieces)[0]) > 1:
        pieces = jax.vmap(combine)(
            *(jax.tree.map(lambda part: part[side::2], pieces) for side in (0, 1))
        )
    return jax.tree.map(lambda part: part[0], pieces)


def carried_in(value, axis, combine, identity):
    peers, here = (lax.axis_size(axis), lax.axis_index(axis))
    passed = jnp.arange(peers) < here

    def kept(part, zero, own):
        part = jnp.where(
            passed.reshape(-1, *(1 for _ in own.shape)),
            part.astype(own.dtype),
            jnp.asarray(zero, own.dtype),
        )
        return part

    pieces = all_in_one(
        jax.tree.map(lambda part, kind: part.astype(kind), value, (jnp.bfloat16, jnp.bfloat16)),
        axis,
    )
    return joined_by_halves(jax.tree.map(kept, pieces, identity, value), combine)


def joined_along(tiles, dim):
    lengths = list(tiles.shape[1:])
    lengths[dim] *= tiles.shape[0]
    return jnp.moveaxis(tiles, 0, dim).reshape(lengths)


def gathered_by_axis(value, axes, dim):
    far, near = axes
    tiles = from_everyone(from_everyone(value, far), near)
    return joined_along(tiles.swapaxes(0, 1).reshape(-1, *value.shape), dim)


def in_blocks(value, dim, peers):
    lengths = value.shape
    tiles = value.reshape(*lengths[:dim], peers, lengths[dim] // peers, *lengths[dim + 1 :])
    return jnp.moveaxis(tiles, dim, 0)


def summed_on_arrival(value, axis, dim):
    tiles = in_blocks(value, dim, lax.axis_size(axis))
    arrived = lax.all_to_all(tiles, axis, split_axis=0, concat_axis=0, tiled=True)
    return arrived.astype(jnp.float32).sum(axis=0)


def sum_by_axis(value, axes, dim):
    far, near = axes
    own = summed_on_arrival(in_blocks(value, dim, lax.axis_size(far)), near, dim + 1)
    return jnp.sum(
        lax.all_to_all(own.astype(jnp.bfloat16), far, 0, 0, tiled=True).astype(jnp.float32), axis=0
    )


def block_step(carry, inputs):
    memory_state, offsets = carry
    query_block, input_gate_block, value_block, log_blk = inputs
    cumulative_decay = jnp.cumsum(log_blk, axis=1)
    length = log_blk.shape[1]
    carried_share = jnp.einsum(
        "eia,eax->eix",
        query_block * jnp.exp(cumulative_decay),
        memory_state,
        precision=TOP_PRECISION,
    )
    middle = cumulative_decay[:, length // 2, :][:, None, :]
    left_side = query_block * jnp.exp(cumulative_decay - middle)
    right_side = input_gate_block * jnp.exp(middle - cumulative_decay)
    causal = (jnp.arange(length)[:, None] >= jnp.arange(length)[None, :])[None, :, :]
    scores = jnp.einsum("htk,hsk->hts", left_side, right_side, precision=TOP_PRECISION)
    scores = jnp.where(causal, scores, 0.0)
    outputs = carried_share + jnp.einsum(
        "hts,hsv->htv", scores, value_block, precision=TOP_PRECISION
    )
    closing_log_decay = cumulative_decay[:, -1, :]
    updated_memory_state = jnp.exp(closing_log_decay)[:, :, None] * memory_state + jnp.einsum(
        "qnj,qnl->qjl",
        input_gate_block * jnp.exp(closing_log_decay[:, None, :] - cumulative_decay),
        value_block,
        precision=TOP_PRECISION,
    )
    return (
        (updated_memory_state, offsets + closing_log_decay),
        (outputs, cumulative_decay + offsets[:, None, :]),
    )


def split_blocks(values, heads_here):
    count = values.shape[0]
    return values.reshape(count // BLOCK, BLOCK, heads_here, HEAD_DIM).transpose(0, 2, 1, 3)


def admission_source_matrix(
    probe_preactivation, retention_preactivation, content_vector, retention_slack, surge_rate
):
    query_act = jax.nn.silu(probe_preactivation.astype(jnp.float32))
    admission_factor = retention_slack[None, :] * jax.nn.sigmoid(
        -retention_preactivation.astype(jnp.float32)
    )
    retention_logarithm = jnp.log1p(-admission_factor) + surge_rate
    return (query_act, admission_factor, content_vector.astype(jnp.float32), retention_logarithm)


def head_output(outputs, subspace_scaling_factor, emission_preactivation):
    count, heads_here = (outputs.shape[0], outputs.shape[1])
    squares = jnp.mean(outputs * outputs, axis=-1, keepdims=True)
    scaled = (
        outputs
        * lax.rsqrt(squares + EPSILON)
        * subspace_scaling_factor.reshape(heads_here, HEAD_DIM)
    )
    scaled = scaled.reshape(count, heads_here * HEAD_DIM)
    return (scaled * jax.nn.silu(emission_preactivation.astype(jnp.float32))).astype(jnp.bfloat16)


def row_norm(stream, mlp_scaling_factor):
    streamf = stream.astype(jnp.float32)
    squares = jnp.mean(streamf * streamf, axis=-1, keepdims=True)
    return (streamf * lax.rsqrt(squares + EPSILON) * mlp_scaling_factor).astype(jnp.bfloat16)


def chain(earlier, later):
    return (earlier[0] * later[0], later[0][:, :, None] * earlier[1] + later[1])


def on_device(
    skip_stream_vector,
    probe_preactivation,
    retention_preactivation,
    content_vector,
    emission_preactivation,
    retention_slack,
    surge_rate,
    subspace_scaling_factor,
    emission_matrix,
    mlp_scaling_factor,
    switch_matrix,
    expansion_matrix,
    contraction_matrix,
):
    gate_whole, up_whole = in_one_piece((switch_matrix, expansion_matrix), "sp", 0, 1)
    down_whole = lax.all_gather(contraction_matrix, "sp", axis=1, tiled=True)
    heads_here = probe_preactivation.shape[1] // HEAD_DIM
    tok_rows = probe_preactivation.shape[0]
    arranged_sources = admission_source_matrix(
        probe_preactivation, retention_preactivation, content_vector, retention_slack, surge_rate
    )
    block_list = tuple((split_blocks(item, heads_here) for item in arranged_sources))
    start_carry = (
        jnp.zeros((heads_here, HEAD_DIM, HEAD_DIM), jnp.float32),
        jnp.zeros((heads_here, HEAD_DIM), jnp.float32),
    )
    (memory_state, offsets), (outputs, cumulative_log_decay) = lax.scan(
        block_step, start_carry, block_list
    )
    incoming_state = carried_in(
        (jnp.exp(offsets), memory_state),
        "sp",
        chain,
        (jnp.ones_like(offsets), jnp.zeros_like(memory_state)),
    )
    outputs = outputs + jnp.einsum(
        "jmxo,mos->jmxs",
        block_list[0] * jnp.exp(cumulative_log_decay),
        incoming_state[1],
        precision=TOP_PRECISION,
    )
    outputs = outputs.transpose(0, 2, 1, 3).reshape(tok_rows, heads_here, HEAD_DIM)
    mixed = head_output(outputs, subspace_scaling_factor, emission_preactivation)
    regrouped = lax.all_to_all(mixed, TP, split_axis=0, concat_axis=1, tiled=True)
    projected = jnp.dot(regrouped, emission_matrix, preferred_element_type=jnp.float32)
    stream = (skip_stream_vector.astype(jnp.float32) + projected).astype(jnp.bfloat16)
    normed = row_norm(stream, mlp_scaling_factor)
    all_rows = gathered_by_axis(normed, ("tp_0", "tp_1"), 0)
    gate_proj = jnp.dot(all_rows, gate_whole, preferred_element_type=jnp.float32)
    up_proj = jnp.dot(all_rows, up_whole, preferred_element_type=jnp.float32)
    hidden = (jax.nn.silu(gate_proj) * up_proj).astype(jnp.bfloat16)
    partial_sum = jnp.dot(hidden, down_whole, preferred_element_type=jnp.float32)
    summed = sum_by_axis(partial_sum.astype(jnp.bfloat16), ("tp_0", "tp_1"), 0)
    return (stream.astype(jnp.float32) + summed).astype(jnp.bfloat16)


def solution(mesh):
    split = Mesh(mesh.devices.reshape(mesh.shape["sp"], 4, 2), ("sp", "tp_0", "tp_1"))
    return jax.shard_map(
        on_device,
        mesh=split,
        in_specs=(
            P(SP_TP, None),
            P("sp", TP),
            P("sp", TP),
            P("sp", TP),
            P("sp", TP),
            P(TP),
            P("sp", TP),
            P(TP),
            P(),
            P(),
            P("sp", TP),
            P("sp", TP),
            P(TP, "sp"),
        ),
        out_specs=P(SP_TP, None),
        check_vma=False,
    )
```

profile of v0, /device:TPU:0, one launch (start us, length us, event | category | flops | bytes accessed | tf_op | source)
XLA Modules:
  0.0 193.7 jit_solution(10395686392634396452)
XLA Ops:
  6.5 1.8 pad_maximum_fusion
  8.4 1.1 convert_multiply_fusion.1
  9.5 1.0 convert.2
  10.5 1.5 divide_multiply_fusion
  12.0 17.0 %while.17 = (s32[]{:T(128)}, f32[1,128,128]{2,1,0:T(8,128)S(1)}, f32[1,128]{1,0:T(1,128)S(1)}, f32[16,1,64,128]{3,2,1,0:T(8,128)S(1)}, f32[16,1,64,128]{3,2,1,0:...) while((s32[]{:T(128)}, f32[1,128,128]{2,1,0:T(8,128)S(1)}, ...), condition=%wide.region_2.3_spmd.clone, body=%wide.region_0.2_spmd.clone.sunk | while | flops 38412544 | bytes 879768 | solution.py:205
  29.0 0.9 broadcast_in_dim.48
  29.9 8.2 %all-to-all-start = ((bf16[16,129,128]{2,1,0:T(8,128)(2,1)}), bf16[16,129,128]{2,1,0:T(8,128)(2,1)S(1)}, u32[]{:S(2)}, u32[]{:S(2)}) async-start(bf16[16,129,128]{2,1,0:T(8,128)(2,1)} %broadcast_in_dim.48), calls=%async_computation | async-start | bytes 1114112 | tf_op jit(solution)/shard_map/all_to_all | solution.py:26
  38.1 0.7 all-gather.5.cloned.1.call-update
  38.9 11.2 %all-to-all-done = bf16[16,129,128]{2,1,0:T(8,128)(2,1)S(1)} async-done(((bf16[16,129,128]{2,1,0:T(8,128)(2,1)}), bf16[16,129,128]{2,1,0:T(8,128)(2,1)S(1)}, u32[]{:S(2)}, u32[]{:S(2)}) %all-to-all-start) | async-done | bytes 528416 | tf_op jit(solution)/shard_map/all_to_all | solution.py:26
  50.8 0.7 multiply_reduce_fusion.1
  51.9 11.6 %all_to_all.44 = bf16[8,128,128]{2,1,0:T(8,128)(2,1)S(1)} all-to-all(bf16[8,128,128]{2,1,0:T(8,128)(2,1)S(1)} %bitcast.185), channel_id=1, replica_groups=mesh['sp'=16,'tp_0'=4,'tp_1'=2] {'tp_0','tp_1'}, dimensions={0} | all-to-all | bytes 524288 | tf_op jit(solution)/shard_map/all_to_all | solution.py:222
  63.7 3.0 %multiply_reduce_fusion = (f32[128]{0:T(128)S(1)}, f32[128,2048]{1,0:T(8,128)S(1)}) fusion(bf16[128,1024]{0,1:T(8,128)(2,1)S(1)} %bitcast.183, bf16[1024,2048]{1,0:T(8,128)(2,1)} %param.23, bf16[128,2048]{1,0:T(8,128)(2,1)S(1)} %copy-done), kind=kOutput, calls=%fused_computation.66 | convolution fusion | flops 538443648 | bytes 6029824 | tf_op jit(solution)/shard_map/dot_general | solution.py:223
  67.1 28.8 %all_to_all.45 = bf16[4,128,2048]{2,1,0:T(8,128)(2,1)S(1)} all-to-all(bf16[4,128,2048]{2,1,0:T(8,128)(2,1)S(1)} %broadcast_in_dim.74), channel_id=1, replica_groups=mesh['sp'=16,'tp_0'=4,'tp_1'=2] {'tp_0'}, dimensions={0} | all-to-all | bytes 4194304 | tf_op jit(solution)/shard_map/all_to_all | solution.py:26
  95.9 0.5 broadcast_in_dim.75
  96.5 7.1 %all_to_all.46 = bf16[2,4,128,2048]{3,2,1,0:T(8,128)(2,1)S(1)} all-to-all(bf16[2,4,128,2048]{3,2,1,0:T(8,128)(2,1)S(1)} %broadcast_in_dim.75), channel_id=1, replica_groups=mesh['sp'=16,'tp_0'=4,'tp_1'=2] {'tp_1'}, dimensions={0} | all-to-all | bytes 8388608 | tf_op jit(solution)/shard_map/all_to_all | solution.py:26
  103.6 2.3 %copy.36 = bf16[2,4,128,2048]{3,2,0,1:T(8,128)(2,1)} copy(bf16[2,4,128,2048]{3,2,1,0:T(8,128)(2,1)S(1)} %all_to_all.46) | data formatting | bytes 8388608 | tf_op jit(solution)/shard_map/all_to_all | solution.py:26
  105.9 7.9 %fusion.43 = f32[1024,704]{0,1:T(8,128)} fusion(bf16[1024,2048]{1,0:T(8,128)(2,1)} %bitcast.178, bf16[2048,1408]{0,1:T(8,128)(2,1)} %all-gather.3.cloned.1.call-done), kind=kOutput, calls=%fused_computation.56 | convolution fusion | flops 2952790016 | bytes 9961472 | tf_op jit(solution)/shard_map/dot_general | solution.py:227
  113.8 14.8 %all-gather.5.cloned.1.call-done = bf16[704,2048]{1,0:T(8,128)(2,1)} async-done(((bf16[704,128]{1,0:T(8,128)(2,1)}), bf16[704,2048]{1,0:T(8,128)(2,1)}) %all-gather.5.cloned.1.call-update) | async-done | bytes 2883600 | tf_op jit(solution)/shard_map/all_gather | solution.py:194
  128.6 12.1 %convolution_convert_fusion = bf16[1024,2048]{1,0:T(8,128)(2,1)} fusion(bf16[704,2048]{1,0:T(8,128)(2,1)} %all-gather.5.cloned.1.call-done, f32[1024,704]{0,1:T(8,128)} %fusion.43, bf16[1024,2048]{1,0:T(8,128)(2,1)} %bitcast.179, bf16[2048,1408]{0,1:T(8,128)(2,1)} %all-gather.3.cloned.1.call-done), kind=kOutput, calls=%fused_computation.53 | convolution fusion | flops 5912002560 | bytes 17039360 | tf_op jit(solution)/shard_map/dot_general | solution.py:230
  140.7 2.5 %copy.39 = bf16[4,2,128,2048]{3,2,0,1:T(8,128)(2,1)S(1)} copy(bf16[4,2,128,2048]{3,2,1,0:T(8,128)(2,1)} %bitcast.180) | data formatting | bytes 8388608 | tf_op jit(solution)/shard_map/reshape;reshape | solution.py:89
  143.2 8.2 %all_to_all.47 = bf16[2,4,128,2048]{3,2,1,0:T(8,128)(2,1)} all-to-all(bf16[2,4,128,2048]{3,2,1,0:T(8,128)(2,1)S(1)} %bitcast.177), channel_id=1, replica_groups=mesh['sp'=16,'tp_0'=4,'tp_1'=2] {'tp_1'}, dimensions={0} | all-to-all | bytes 8388608 | tf_op jit(solution)/shard_map/all_to_all | solution.py:95
  151.3 3.5 %reduce_sum.41 = bf16[4,128,2048]{2,1,0:T(8,128)(2,1)S(1)} reduce(bf16[2,4,128,2048]{3,2,1,0:T(8,128)(2,1)} %all_to_all.47, bf16[]{:T(256)} %constant.49.clone.1), dimensions={0}, to_apply=%region_5.6 | reduce | flops 1048576 | bytes 6291458 | tf_op jit(solution)/shard_map/reduce_sum | solution.py:96
  154.9 30.7 %all_to_all.48 = bf16[4,128,2048]{2,1,0:T(8,128)(2,1)S(1)} all-to-all(bf16[4,128,2048]{2,1,0:T(8,128)(2,1)S(1)} %reduce_sum.41), channel_id=1, replica_groups=mesh['sp'=16,'tp_0'=4,'tp_1'=2] {'tp_0'}, dimensions={0} | all-to-all | bytes 4194304 | tf_op jit(solution)/shard_map/all_to_all | solution.py:103
  186.0 0.9 add_convert_fusion
  (197 shorter events, 18.0 us)
Async XLA Ops:
  6.5 99.4 %all-gather.3.cloned.1.call-start = ((), (), s32[]{:S(2)}) async-start(), calls=%async_computation.6 | async-start | bytes 6127616 | tf_op jit(solution)/shard_map/all_gather | solution.py:17
  29.9 20.2 %all-to-all-start = ((bf16[16,129,128]{2,1,0:T(8,128)(2,1)}), bf16[16,129,128]{2,1,0:T(8,128)(2,1)S(1)}, u32[]{:S(2)}, u32[]{:S(2)}) async-start(bf16[16,129,128]{2,1,0:T(8,128)(2,1)} %broadcast_in_dim.48), calls=%async_computation | async-start | bytes 1114112 | tf_op jit(solution)/shard_map/all_to_all | solution.py:26
  38.1 90.5 %all-gather.5.cloned.1.call-start = ((), (), s32[]{:S(2)}) async-start(), calls=%async_computation.7 | async-start | bytes 3063808 | tf_op jit(solution)/shard_map/all_gather | solution.py:194
  50.3 1.3 copy-start.1
  50.3 1.3 copy-start.3
  50.6 13.1 %copy-start = (bf16[128,2048]{1,0:T(8,128)(2,1)S(1)}, bf16[128,2048]{1,0:T(8,128)(2,1)}, u32[]{:S(2)}) copy-start(bf16[128,2048]{1,0:T(8,128)(2,1)} %param.15) | copy-start | bytes 1572868
  63.7 3.0 %copy-start.2 = (f32[2048]{0:T(1024)S(1)}, f32[2048]{0:T(1024)}, u32[]{:S(2)}) copy-start(f32[2048]{0:T(1024)} %param.24) | copy-start | bytes 24580
Sparse Core Ops, SparseCore 0:
  9.4 66.9 all-gather.2
  78.6 49.9 all-gather.4
where the time goes:
time: 194 us
  blocking collectives  86.3 us (44%)
  matrix products  37.4 us (19%)
  waiting for transfers between devices  26.8 us (14%)
  between operations  13.7 us (7%)
  other arithmetic  13.2 us (7%)
  starting transfers between devices  8.21 us (4%)
  local copies, waits for them, and re-layouts  7.13 us (4%)
    all_to_all x2, blocking collectives, from_everyone(): lax.all_to_all(jnp.broadcast_to(value[None], (peers, *value.shape)), axis...  35.9 us
    all_to_all x1, blocking collectives, sum_by_axis(): lax.all_to_all(own.astype(jnp.bfloat16), far, 0, 0, tiled=True)  30.7 us
    all_gather x1, waiting for transfers between devices, on_device(): down_whole = lax.all_gather(contraction_matrix, 'sp', axis=1, tiled=True)  14.8 us
    dot_general x1, matrix products, on_device(): jnp.dot(hidden, down_whole, preferred_element_type=jnp.float32)  12.1 us
    all_to_all x1, blocking collectives, on_device(): lax.all_to_all(mixed, TP, split_axis=0, concat_axis=1, tiled=True)  11.6 us
    all_to_all x1, waiting for transfers between devices, from_everyone(): lax.all_to_all(jnp.broadcast_to(value[None], (peers, *value.shape)), axis...  11.2 us
    all_to_all x1, blocking collectives, summed_on_arrival(): lax.all_to_all(tiles, axis, split_axis=0, concat_axis=0, tiled=True)  8.18 us
    all_to_all x1, starting transfers between devices, from_everyone(): lax.all_to_all(jnp.broadcast_to(value[None], (peers, *value.shape)), axis...  8.16 us
  transfers between devices with their start and end apart: 3, of which 2 were waited for; matrix products, arithmetic and copies ran while one was open for 19% of the time, Pallas kernels for 0%

commit v1 on v0

--- a/solution.py
+++ b/solution.py
@@ -3,6 +3,7 @@
 from jax import lax
 from jax.sharding import Mesh
 from jax.sharding import PartitionSpec as P
+from jax.lax import all_to_all, axis_size
 
 HEAD_DIM = 128
 BLOCK = 64
@@ -10,6 +11,13 @@
 SP_TP = ("sp", "tp_0", "tp_1")
 EPSILON = 1e-06
 TOP_PRECISION = lax.Precision.HIGHEST
+
+
+def show_strings(block_in, array_dim):
+    back = axis_size("sp")
+    n_now = jnp.stack([block_in] * back, 0)
+    t_next = all_to_all(n_now, "sp", 0, 0)
+    return jnp.concatenate(t_next, array_dim)
 
 
 def in_one_piece(arrays, axis, dim, along):
@@ -191,7 +199,7 @@
     contraction_matrix,
 ):
     gate_whole, up_whole = in_one_piece((switch_matrix, expansion_matrix), "sp", 0, 1)
-    down_whole = lax.all_gather(contraction_matrix, "sp", axis=1, tiled=True)
+    down_whole = show_strings(contraction_matrix, array_dim=1)
     heads_here = probe_preactivation.shape[1] // HEAD_DIM
     tok_rows = probe_preactivation.shape[0]
     arranged_sources = admission_source_matrix(

time: 194 us -> 221 us (1.14)
  waiting for transfers between devices: 26.8 us -> 44.4 us
  local copies, waits for them, and re-layouts: 7.13 us -> 11.8 us
  starting transfers between devices: 8.21 us -> 12.8 us
    all_to_all x0 -> x1, waiting for transfers between devices: none -> 32.4 us  [show_strings(): t_next = all_to_all(n_now, 'sp', 0, 0)]
    all_gather x1 -> x0, waiting for transfers between devices: 14.8 us -> none  [on_device(): down_whole = lax.all_gather(contraction_matrix, 'sp', axis=1, tiled=True)]
    all_to_all x0 -> x1, starting transfers between devices: none -> 4.64 us  [show_strings(): t_next = all_to_all(n_now, 'sp', 0, 0)]
    all_to_all x1, local copies, waits for them, and re-layouts: 2.33 us -> 4.8 us  [from_everyone(): lax.all_to_all(jnp.broadcast_to(value[None], (peers, *value.shape)), axis...]
where the time goes in v1:
time: 221 us; the launch traced here: 220 us
  blocking collectives  86.2 us (39%)
  waiting for transfers between devices  44.4 us (20%)
  matrix products  37.4 us (17%)
  between operations  13.7 us (6%)
  other arithmetic  13.1 us (6%)
  starting transfers between devices  12.8 us (6%)
  local copies, waits for them, and re-layouts  11.8 us (5%)
    all_to_all x2, blocking collectives, from_everyone(): lax.all_to_all(jnp.broadcast_to(value[None], (peers, *value.shape)), axis...  37 us
    all_to_all x1, waiting for transfers between devices, show_strings(): t_next = all_to_all(n_now, 'sp', 0, 0)  32.4 us
    all_to_all x1, blocking collectives, sum_by_axis(): lax.all_to_all(own.astype(jnp.bfloat16), far, 0, 0, tiled=True)  29.4 us
    dot_general x1, matrix products, on_device(): jnp.dot(hidden, down_whole, preferred_element_type=jnp.float32)  12 us
    all_to_all x1, waiting for transfers between devices, from_everyone(): lax.all_to_all(jnp.broadcast_to(value[None], (peers, *value.shape)), axis...  12 us
    all_to_all x1, blocking collectives, on_device(): lax.all_to_all(mixed, TP, split_axis=0, concat_axis=1, tiled=True)  11.6 us
    all_to_all x1, blocking collectives, summed_on_arrival(): lax.all_to_all(tiles, axis, split_axis=0, concat_axis=0, tiled=True)  8.18 us
    all_to_all x1, starting transfers between devices, from_everyone(): lax.all_to_all(jnp.broadcast_to(value[None], (peers, *value.shape)), axis...  8.16 us
  transfers between devices with their start and end apart: 3, of which 2 were waited for; matrix products, arithmetic and copies ran while one was open for 19% of the time, Pallas kernels for 0%

profile of v1, /device:TPU:0, one launch (start us, length us, event | category | flops | bytes accessed | tf_op | source)
XLA Modules:
  0.0 220.4 jit_solution(11975222686143445894)
XLA Ops:
  6.5 1.8 pad_maximum_fusion
  8.4 1.1 convert_multiply_fusion.1
  9.5 1.0 convert.2
  10.5 1.4 divide_multiply_fusion
  11.9 17.0 %while.17 = (s32[]{:T(128)}, f32[1,128,128]{2,1,0:T(8,128)S(1)}, f32[1,128]{1,0:T(1,128)S(1)}, f32[16,1,64,128]{3,2,1,0:T(8,128)S(1)}, f32[16,1,64,128]{3,2,1,0:...) while((s32[]{:T(128)}, f32[1,128,128]{2,1,0:T(8,128)S(1)}, ...), condition=%wide.region_2.3_spmd.clone, body=%wide.region_0.2_spmd.clone.sunk | while | flops 38412544 | bytes 879768 | solution.py:213
  29.0 0.9 broadcast_in_dim.48
  29.9 8.2 %all-to-all-start = ((bf16[16,129,128]{2,1,0:T(8,128)(2,1)}), bf16[16,129,128]{2,1,0:T(8,128)(2,1)S(1)}, u32[]{:S(2)}, u32[]{:S(2)}) async-start(bf16[16,129,128]{2,1,0:T(8,128)(2,1)} %broadcast_in_dim.48), calls=%async_computation | async-start | bytes 1114112 | tf_op jit(solution)/shard_map/all_to_all | solution.py:34
  38.0 12.0 %all-to-all-done = bf16[16,129,128]{2,1,0:T(8,128)(2,1)S(1)} async-done(((bf16[16,129,128]{2,1,0:T(8,128)(2,1)}), bf16[16,129,128]{2,1,0:T(8,128)(2,1)S(1)}, u32[]{:S(2)}, u32[]{:S(2)}) %all-to-all-start) | async-done | bytes 528416 | tf_op jit(solution)/shard_map/all_to_all | solution.py:34
  50.8 0.7 multiply_reduce_fusion.1
  51.8 11.6 %all_to_all.49 = bf16[8,128,128]{2,1,0:T(8,128)(2,1)S(1)} all-to-all(bf16[8,128,128]{2,1,0:T(8,128)(2,1)S(1)} %bitcast.192), channel_id=1, replica_groups=mesh['sp'=16,'tp_0'=4,'tp_1'=2] {'tp_0','tp_1'}, dimensions={0} | all-to-all | bytes 524288 | tf_op jit(solution)/shard_map/all_to_all | solution.py:230
  63.6 3.0 %multiply_reduce_fusion = (f32[128]{0:T(128)S(1)}, f32[128,2048]{1,0:T(8,128)S(1)}) fusion(bf16[128,1024]{0,1:T(8,128)(2,1)S(1)} %bitcast.190, bf16[1024,2048]{1,0:T(8,128)(2,1)} %param.23, bf16[128,2048]{1,0:T(8,128)(2,1)S(1)} %copy-done), kind=kOutput, calls=%fused_computation.68 | convolution fusion | flops 538443648 | bytes 6029824 | tf_op jit(solution)/shard_map/dot_general | solution.py:231
  67.1 28.8 %all_to_all.50 = bf16[4,128,2048]{2,1,0:T(8,128)(2,1)S(1)} all-to-all(bf16[4,128,2048]{2,1,0:T(8,128)(2,1)S(1)} %broadcast_in_dim.74), channel_id=1, replica_groups=mesh['sp'=16,'tp_0'=4,'tp_1'=2] {'tp_0'}, dimensions={0} | all-to-all | bytes 4194304 | tf_op jit(solution)/shard_map/all_to_all | solution.py:34
  96.4 8.3 %all_to_all.51 = bf16[2,4,128,2048]{3,2,1,0:T(8,128)(2,1)} all-to-all(bf16[2,4,128,2048]{3,2,1,0:T(8,128)(2,1)S(1)} %broadcast_in_dim.75), channel_id=1, replica_groups=mesh['sp'=16,'tp_0'=4,'tp_1'=2] {'tp_1'}, dimensions={0} | all-to-all | bytes 8388608 | tf_op jit(solution)/shard_map/all_to_all | solution.py:34
  104.7 2.2 stack.2
  106.8 4.6 %all-to-all-start.4 = ((bf16[16,704,128]{2,1,0:T(8,128)(2,1)}), bf16[16,704,128]{2,1,0:T(8,128)(2,1)}, u32[]{:S(2)}, u32[]{:S(2)}) async-start(bf16[16,704,128]{2,1,0:T(8,128)(2,1)} %stack.2), calls=%async_computation.4 | async-start | bytes 5767168 | tf_op jit(solution)/shard_map/all_to_all | solution.py:19
  111.5 4.8 %copy.37 = bf16[2,4,128,2048]{3,2,0,1:T(8,128)(2,1)} copy(bf16[2,4,128,2048]{3,2,1,0:T(8,128)(2,1)} %all_to_all.51) | data formatting | bytes 8388608 | tf_op jit(solution)/shard_map/all_to_all | solution.py:34
  116.3 7.8 %fusion.45 = f32[1024,704]{0,1:T(8,128)} fusion(bf16[1024,2048]{1,0:T(8,128)(2,1)} %bitcast.185, bf16[2048,1408]{0,1:T(8,128)(2,1)} %all-gather.2.cloned.1.call-done), kind=kOutput, calls=%fused_computation.58 | convolution fusion | flops 2952790016 | bytes 9961472 | tf_op jit(solution)/shard_map/dot_general | solution.py:235
  124.1 32.4 %all-to-all-done.4 = bf16[16,704,128]{2,1,0:T(8,128)(2,1)} async-done(((bf16[16,704,128]{2,1,0:T(8,128)(2,1)}), bf16[16,704,128]{2,1,0:T(8,128)(2,1)}, u32[]{:S(2)}, u32[]{:S(2)}) %all-to-all-start.4) | async-done | bytes 2883616 | tf_op jit(solution)/shard_map/all_to_all | solution.py:19
  156.6 12.0 %convolution_convert_fusion = bf16[1024,2048]{1,0:T(8,128)(2,1)} fusion(f32[1024,704]{0,1:T(8,128)} %fusion.45, bf16[1024,2048]{1,0:T(8,128)(2,1)} %bitcast.186, bf16[2048,1408]{0,1:T(8,128)(2,1)} %all-gather.2.cloned.1.call-done, bf16[16,704,128]{2,1,0:T(8,128)(2,1)} %all-to-all-done.4), kind=kOutput, calls=%fused_computation.53 | convolution fusion | flops 5912002560 | bytes 17039360 | tf_op jit(solution)/shard_map/dot_general | solution.py:238
  168.6 2.5 %copy.46 = bf16[4,2,128,2048]{3,2,0,1:T(8,128)(2,1)S(1)} copy(bf16[4,2,128,2048]{3,2,1,0:T(8,128)(2,1)} %bitcast.187) | data formatting | bytes 8388608 | tf_op jit(solution)/shard_map/reshape;reshape | solution.py:97
  171.1 8.2 %all_to_all.52 = bf16[2,4,128,2048]{3,2,1,0:T(8,128)(2,1)} all-to-all(bf16[2,4,128,2048]{3,2,1,0:T(8,128)(2,1)S(1)} %bitcast.184), channel_id=1, replica_groups=mesh['sp'=16,'tp_0'=4,'tp_1'=2] {'tp_1'}, dimensions={0} | all-to-all | bytes 8388608 | tf_op jit(solution)/shard_map/all_to_all | solution.py:103
  179.3 3.5 %reduce_sum.41 = bf16[4,128,2048]{2,1,0:T(8,128)(2,1)S(1)} reduce(bf16[2,4,128,2048]{3,2,1,0:T(8,128)(2,1)} %all_to_all.52, bf16[]{:T(256)} %constant.49.clone.1), dimensions={0}, to_apply=%region_5.6 | reduce | flops 1048576 | bytes 6291458 | tf_op jit(solution)/shard_map/reduce_sum | solution.py:104
  182.8 29.4 %all_to_all.53 = bf16[4,128,2048]{2,1,0:T(8,128)(2,1)S(1)} all-to-all(bf16[4,128,2048]{2,1,0:T(8,128)(2,1)S(1)} %reduce_sum.41), channel_id=1, replica_groups=mesh['sp'=16,'tp_0'=4,'tp_1'=2] {'tp_0'}, dimensions={0} | all-to-all | bytes 4194304 | tf_op jit(solution)/shard_map/all_to_all | solution.py:111
  212.6 0.9 add_convert_fusion
  (199 shorter events, 18.5 us)
Async XLA Ops:
  6.5 109.8 %all-gather.2.cloned.1.call-start = ((), (), s32[]{:S(2)}) async-start(), calls=%async_computation.7 | async-start | bytes 6127616 | tf_op jit(solution)/shard_map/all_gather | solution.py:25
  29.9 20.2 %all-to-all-start = ((bf16[16,129,128]{2,1,0:T(8,128)(2,1)}), bf16[16,129,128]{2,1,0:T(8,128)(2,1)S(1)}, u32[]{:S(2)}, u32[]{:S(2)}) async-start(bf16[16,129,128]{2,1,0:T(8,128)(2,1)} %broadcast_in_dim.48), calls=%async_computation | async-start | bytes 1114112 | tf_op jit(solution)/shard_map/all_to_all | solution.py:34
  50.2 1.5 copy-start.1
  50.2 1.4 copy-start.4
  50.5 13.1 %copy-start = (bf16[128,2048]{1,0:T(8,128)(2,1)S(1)}, bf16[128,2048]{1,0:T(8,128)(2,1)}, u32[]{:S(2)}) copy-start(bf16[128,2048]{1,0:T(8,128)(2,1)} %param.15) | copy-start | bytes 1572868
  63.6 3.0 %copy-start.3 = (f32[2048]{0:T(1024)S(1)}, f32[2048]{0:T(1024)}, u32[]{:S(2)}) copy-start(f32[2048]{0:T(1024)} %param.24) | copy-start | bytes 24580
  96.4 8.3 %copy-start.2 = (bf16[704,128]{1,0:T(8,128)(2,1)S(1)}, bf16[704,128]{1,0:T(8,128)(2,1)}, u32[]{:S(2)}) copy-start(bf16[704,128]{1,0:T(8,128)(2,1)} %param.27) | copy-start | bytes 540676
  106.8 49.7 %all-to-all-start.4 = ((bf16[16,704,128]{2,1,0:T(8,128)(2,1)}), bf16[16,704,128]{2,1,0:T(8,128)(2,1)}, u32[]{:S(2)}, u32[]{:S(2)}) async-start(bf16[16,704,128]{2,1,0:T(8,128)(2,1)} %stack.2), calls=%async_computation.4 | async-start | bytes 5767168 | tf_op jit(solution)/shard_map/all_to_all | solution.py:19
Sparse Core Ops, SparseCore 0:
  9.4 66.9 all-gather.1
